TPU v7x, 32 devices: a whole 2x2x4 slice. The times are simulated.
32 devices in a mesh: sp: 16 (over z, y, core), tp: 2 (over x).
Axes of the slice: x: 2, y: 2, z: 4, core: 2. Of those that a mesh axis runs over, the one named last changes fastest.
Arguments:
- activations: bfloat16 [4096, 2048], P('sp', 'tp'), may hold values from -8 to 8
- norm_gain: float32 [2048], replicated, may hold values from 0.1 to 1.9
- win_query: bfloat16 [2048, 1024], P(None, 'tp'), may hold values from -1 to 1
- win_key: bfloat16 [2048, 512], P(None, 'tp'), may hold values from -1 to 1
- win_value: bfloat16 [2048, 512], P(None, 'tp'), may hold values from -0.125 to 0.125
- sink_logit: float32 [16], P('tp'), may hold values from 1 to 6
- lat_query: bfloat16 [2048, 1536], P(None, 'tp'), may hold values from -1 to 1
- key_value_down_weight: bfloat16 [2048, 128], replicated, may hold values from -0.125 to 0.125
- rope_key: bfloat16 [2048, 64], replicated, may hold values from -1 to 1
- latent_norm_gain: float32 [128], replicated, may hold values from 0.1 to 1.9
- key_up_weight: bfloat16 [128, 1024], P(None, 'tp'), may hold values from -0.5 to 0.5
- value_up_weight: bfloat16 [128, 1024], P(None, 'tp'), may hold values from -0.5 to 0.5
- out_win: bfloat16 [1024, 2048], P('tp'), may hold values from -0.359375 to 0.359375
- out_lat: bfloat16 [1024, 2048], P('tp'), may hold values from -0.59765625 to 0.59765625
Outputs:
- mixed: bfloat16 [4096, 2048], P('sp', 'tp')
All inputs are finite; a program needn't handle non-finite values.
Results may differ from a plain program's by a relative error of at most 0.025.
Values may be sent and summed in bfloat16 or wider, within the bound.
A program may use at most 64 MiB of HBM per device.

v0:
```python
import functools

import jax
import jax.numpy as jnp
import numpy as np
from jax import lax
from jax.experimental import pallas as pl
from jax.experimental.pallas import tpu as pltpu
from jax.sharding import PartitionSpec as P

HEADS_A = 16
DH = 64
WINDOW = 128
UNROTATED_WIDTH = 128
D_ROPE = 64
VALUE_WIDTH = 128

EPSILON = 1e-06
ROPE_BASE = 10000.0
LOG2E = 1.4426950408889634
MESH = pl.DeviceIdType.MESH
F32 = jnp.float32
BF16 = jnp.bfloat16
SUB = 2
BANDS = 4


def turn(vectors, cosine, sine):
    half = vectors.shape[-1] // 2
    swapped = jnp.concatenate([vectors[:, half:], vectors[:, :half]], axis=1)
    return vectors * cosine + swapped * sine


def dot_nt(a, b):
    return lax.dot_general(a, b, (((1,), (1,)), ((), ())), preferred_element_type=F32)


def project_kernel(
    n_sp, n_tp,
    x_ref, gain_ref, near_ref, base_ref, sink_ref, lng_ref, kup_ref,
    wkv_hbm, wr_hbm, wk_hbm, wv_hbm, wq_hbm, wlq_hbm,
    q_ref, kv_ref, win_ref,
    x_all, wkv, wr, wk, wv, wq, wlq, akv, ar, ak, av, aq, alq, sq, gath, halo, qwin,
    w_sem, x_send, x_recv, z_send, z_recv, y_send, y_recv, c_send, c_recv, h_send, h_recv,
):
    sp = lax.axis_index("sp")
    tp = lax.axis_index("tp")
    rows, local = x_ref.shape
    part = local // SUB
    hi = n_sp // 4
    z, y, c = sp // 4, (sp // 2) % 2, sp % 2

    def at(zz, yy, cc):
        return (zz * 2 + yy) * 2 + cc

    right, left = (sp + 1) % n_sp, (sp + n_sp - 1) % n_sp

    weights = ((wkv_hbm, wkv), (wr_hbm, wr), (wk_hbm, wk), (wv_hbm, wv), (wq_hbm, wq), (wlq_hbm, wlq))
    loads = [pltpu.make_async_copy(a, b, w_sem.at[i]) for i, (a, b) in enumerate(weights)]
    for load in loads:
        load.start()

    barrier = pltpu.get_barrier_semaphore()
    peers = [(sp, (tp + s) % n_tp) for s in range(1, n_tp)]
    peers += [(at((z + d) % hi, y, c), tp) for d in range(1, hi)]
    peers += [(at(z, 1 - y, c), tp), (at(z, y, 1 - c), tp), (right, tp), (left, tp)]
    for peer in peers:
        pl.semaphore_signal(barrier, inc=1, device_id=peer, device_id_type=MESH)
    pl.semaphore_wait(barrier, len(peers))

    def remote(src, dst, send, recv, device):
        return pltpu.make_async_remote_copy(
            src_ref=src, dst_ref=dst, send_sem=send, recv_sem=recv, device_id=device, device_id_type=MESH
        )

    x_copies = {}
    for cc in range(SUB):
        for s in range(1, n_tp):
            x_copies[s, cc] = remote(
                x_ref.at[:, cc * part : (cc + 1) * part],
                x_all.at[tp * SUB + cc],
                x_send.at[s, cc],
                x_recv.at[s, cc],
                (sp, (tp + s) % n_tp),
            )
            x_copies[s, cc].start()

    def add_in(block, slot, pairs, first):
        where = pl.ds(pl.multiple_of(slot * part, part), part)
        for weight, acc in pairs:
            if weight is wr:
                term = dot_nt(block, weight[:, where])
            else:
                term = jnp.dot(block, weight[where, :], preferred_element_type=F32)
            acc[...] = term if first else acc[...] + term

    def norm_block(raw, slot, first):
        wide = raw.astype(F32)
        total = jnp.broadcast_to(jnp.sum(wide * wide, axis=1, keepdims=True), sq.shape)
        sq[...] = total if first else sq[...] + total
        return (wide * gain_ref[slot]).astype(BF16)

    near_cos, near_sin = near_ref[0], near_ref[1]
    base_cos, base_sin = base_ref[sp, 0:1, :], base_ref[sp, 1:2, :]
    cosine = near_cos * base_cos - near_sin * base_sin
    plain_sine = near_sin * base_cos + near_cos * base_sin
    lane = lax.broadcasted_iota(jnp.int32, plain_sine.shape, 1)
    sine = jnp.where(lane < D_ROPE // 2, -plain_sine, plain_sine)
    small = ((wkv, akv), (wr, ar))
    big = ((wk, ak), (wv, av), (wq, aq), (wlq, alq))
    for load in loads:
        load.wait()
    for cc in range(SUB):
        slot = tp * SUB + cc
        block = norm_block(x_ref[:, cc * part : (cc + 1) * part], slot, cc == 0)
        add_in(block, slot, small + big, cc == 0)
    steps = [(s, cc) for cc in range(SUB) for s in range(1, n_tp)]
    for s, cc in steps[:-1]:
        x_copies[s, cc].wait_recv()
        slot = ((tp + n_tp - s) % n_tp) * SUB + cc
        add_in(norm_block(x_all[slot], slot, False), slot, small + big, False)
    s, cc = steps[-1]
    x_copies[s, cc].wait_recv()
    last_slot = ((tp + n_tp - s) % n_tp) * SUB + cc
    last_block = norm_block(x_all[last_slot], last_slot, False)
    add_in(last_block, last_slot, small, False)

    scale = lax.rsqrt(sq[:, 0:1] / (local * n_tp) + EPSILON)
    comp = akv[...]
    latent = comp * lax.rsqrt(jnp.mean(comp * comp, axis=1, keepdims=True) + EPSILON) * lng_ref[...]
    rotary = turn(ar[...] * scale, cosine, sine)
    gath[sp, 0:rows, :] = latent.astype(BF16)
    gath[sp, rows : rows + rows // 2, :] = jnp.concatenate(
        [rotary[: rows // 2], rotary[rows // 2 :]], axis=1
    ).astype(BF16)

    def forward(block, sends, recvs, index, device):
        copy = remote(gath.at[block], gath.at[block], sends.at[index], recvs.at[index], device)
        copy.start()
        return copy

    to_y, to_c = (at(z, 1 - y, c), tp), (at(z, y, 1 - c), tp)
    z_copies = [forward(sp, z_send, z_recv, d, (at((z + d) % hi, y, c), tp)) for d in range(1, hi)]
    y_copies = [forward(sp, y_send, y_recv, 0, to_y)]
    c_copies = [forward(sp, c_send, c_recv, 0, to_c)]

    add_in(last_block, last_slot, big, False)
    k_cols = ak.shape[1]
    halo[WINDOW : WINDOW + rows, 0:k_cols] = (ak[...] * scale).astype(BF16)
    halo[WINDOW : WINDOW + rows, k_cols : 2 * k_cols] = (av[...] * scale).astype(BF16)
    h_copies = [
        remote(halo.at[rows : rows + WINDOW], halo.at[0:WINDOW], h_send.at[0], h_recv.at[0], (right, tp)),
        remote(
            halo.at[WINDOW : 2 * WINDOW],
            halo.at[rows + WINDOW : rows + 2 * WINDOW],
            h_send.at[1],
            h_recv.at[1],
            (left, tp),
        ),
    ]
    for copy in h_copies:
        copy.start()
    qwin[...] = (aq[...] * scale).astype(BF16)
    per_head = UNROTATED_WIDTH + D_ROPE
    factor = per_head ** (-0.5) * LOG2E
    for h in range(alq.shape[1] // per_head):
        one = alq[:, h * per_head : (h + 1) * per_head] * scale
        plain = one[:, :UNROTATED_WIDTH].astype(BF16)
        seen = dot_nt(plain, kup_ref[:, h * UNROTATED_WIDTH : (h + 1) * UNROTATED_WIDTH]) * factor
        turned = turn(one[:, UNROTATED_WIDTH:], cosine, sine) * factor
        q_ref[h, :, 0:UNROTATED_WIDTH] = seen.astype(BF16)
        q_ref[h, :, UNROTATED_WIDTH:] = jnp.concatenate([turned, jnp.zeros_like(turned)], axis=1).astype(BF16)

    for d in range(1, hi):
        z_copies[d - 1].wait_recv()
        block = at((z + hi - d) % hi, y, c)
        y_copies.append(forward(block, y_send, y_recv, d, to_y))
        c_copies.append(forward(block, c_send, c_recv, d, to_c))
    for copy in h_copies:
        copy.wait()

    span = 3 * WINDOW
    spots = lax.broadcasted_iota(jnp.int32, (WINDOW, span), 0)
    keys_at = lax.broadcasted_iota(jnp.int32, (WINDOW, span), 1)
    distance = jnp.abs(spots + WINDOW - keys_at)
    far = distance.astype(F32)
    seq_total = rows * n_sp

    def window(kv_head):
        for b in range(rows // WINDOW):
            key_pos = sp * rows + (b - 1) * WINDOW + keys_at
            inside = (distance <= WINDOW) & (key_pos >= 0) & (key_pos < seq_total)
            keys = halo[b * WINDOW : b * WINDOW + span, kv_head * DH : (kv_head + 1) * DH]
            values = halo[b * WINDOW : b * WINDOW + span, k_cols + kv_head * DH : k_cols + (kv_head + 1) * DH]
            pieces = []
            for g in range(2):
                head = kv_head * 2 + g
                query = qwin[b * WINDOW : (b + 1) * WINDOW, head * DH : (head + 1) * DH]
                place = (tp * sink_ref.shape[0] + head + 1).astype(F32)
                slope = jnp.exp2(jnp.full((1, span), -8.0 / HEADS_A, F32) * place)
                scores = dot_nt(query, keys) * DH ** (-0.5) - slope * far
                scores = jnp.where(inside, scores, -jnp.inf)
                peak = jnp.maximum(jnp.max(scores, axis=1, keepdims=True), sink_ref[head])
                weight = jnp.exp(scores - peak)
                bottom = jnp.sum(weight, axis=1, keepdims=True) + jnp.exp(sink_ref[head] - peak)
                blended = jnp.dot(weight.astype(BF16), values, preferred_element_type=F32)
                pieces.append(blended / bottom)
            win_ref[b * WINDOW : (b + 1) * WINDOW, kv_head * 2 * DH : (kv_head + 1) * 2 * DH] = (
                jnp.concatenate(pieces, axis=1).astype(BF16)
            )

    kv_heads = k_cols // DH
    for kv_head in range((kv_heads + 1) // 2):
        window(kv_head)
    for d in range(hi):
        y_copies[d].wait_recv()
        c_copies.append(forward(at((z + hi - d) % hi, 1 - y, c), c_send, c_recv, hi + d, to_c))
    for kv_head in range((kv_heads + 1) // 2, kv_heads):
        window(kv_head)

    lanes = lax.broadcasted_iota(jnp.int32, (rows // 2, D_ROPE), 1)
    mark = jnp.where(lanes == 0, 1.0, 0.0).astype(BF16)

    def assemble(block):
        base = pl.multiple_of(block * rows, rows)
        kv_ref[pl.ds(base, rows), 0:UNROTATED_WIDTH] = gath[block, 0:rows, :]
        both = gath[block, rows : rows + rows // 2, :]
        kv_ref[pl.ds(base, rows // 2), UNROTATED_WIDTH:] = jnp.concatenate([both[:, :D_ROPE], mark], axis=1)
        kv_ref[pl.ds(base + rows // 2, rows // 2), UNROTATED_WIDTH:] = jnp.concatenate(
            [both[:, D_ROPE:], mark], axis=1
        )

    for d in range(hi):
        assemble(at((z + hi - d) % hi, y, c))
        assemble(at((z + hi - d) % hi, 1 - y, c))
    for d in range(hi):
        c_copies[d].wait_recv()
        assemble(at((z + hi - d) % hi, y, 1 - c))
    for d in range(hi):
        c_copies[hi + d].wait_recv()
        assemble(at((z + hi - d) % hi, 1 - y, 1 - c))
    for copy in list(x_copies.values()) + z_copies + y_copies + c_copies:
        copy.wait_send()


def attend_kernel(
    n_tp,
    q_ref, kv_ref, win_ref, vup_ref, ow_hbm, ol_hbm,
    out_ref,
    ow, ol, acc, peak, lat, outgoing, incoming, own, w_sem, send, recv,
):
    sp = lax.axis_index("sp")
    tp = lax.axis_index("tp")
    heads, rows, _ = q_ref.shape
    half = rows // BANDS
    cols = out_ref.shape[1]
    loads = [pltpu.make_async_copy(ow_hbm, ow, w_sem.at[0]), pltpu.make_async_copy(ol_hbm, ol, w_sem.at[1])]
    for load in loads:
        load.start()
    barrier = pltpu.get_barrier_semaphore()
    for s in range(1, n_tp):
        pl.semaphore_signal(barrier, inc=1, device_id=(sp, (tp + s) % n_tp), device_id_type=MESH)
    pl.semaphore_wait(barrier, n_tp - 1)

    chunk = min(1024, kv_ref.shape[0])
    copies = []
    for b in range(BANDS):
        query = jnp.concatenate([q_ref[h, b * half : (b + 1) * half, :] for h in range(heads)], axis=0)
        acc[...] = jnp.zeros_like(acc)
        peak[...] = jnp.full_like(peak, -jnp.inf)

        def step(i, carry):
            keys = kv_ref[pl.ds(i * chunk if isinstance(i, int) else pl.multiple_of(i * chunk, chunk), chunk), :]
            scores = dot_nt(query, keys)
            old = peak[:, 0:1]
            new = jnp.maximum(old, jnp.max(scores, axis=1, keepdims=True))
            weight = jnp.exp2(scores - new).astype(BF16)
            acc[...] = acc[...] * jnp.exp2(old - new) + jnp.dot(weight, keys, preferred_element_type=F32)
            peak[...] = jnp.broadcast_to(new, peak.shape)
            return carry

        count = kv_ref.shape[0] // chunk
        if count > 4:
            lax.fori_loop(0, count, step, 0)
        else:
            for i in range(count):
                step(i, 0)
        bottom = acc[:, UNROTATED_WIDTH + D_ROPE : UNROTATED_WIDTH + D_ROPE + 1]
        blended = (acc[:, 0:VALUE_WIDTH] / bottom).astype(BF16)
        for h in range(heads):
            where = slice(h * VALUE_WIDTH, (h + 1) * VALUE_WIDTH)
            lat[:, where] = jnp.dot(
                blended[h * half : (h + 1) * half], vup_ref[:, where], preferred_element_type=F32
            ).astype(BF16)
        if b == 0:
            for load in loads:
                load.wait()
        won = win_ref[b * half : (b + 1) * half, :]

        def terms(j):
            where = pl.ds(pl.multiple_of(j * cols, cols), cols)
            return jnp.dot(won, ow[:, where], preferred_element_type=F32) + jnp.dot(
                lat[...], ol[:, where], preferred_element_type=F32
            )

        for s in range(1, n_tp):
            other = (tp + s) % n_tp
            outgoing[b, s - 1] = terms(other).astype(BF16)
            copy = pltpu.make_async_remote_copy(
                src_ref=outgoing.at[b, s - 1],
                dst_ref=incoming.at[b, s - 1],
                send_sem=send.at[b, s],
                recv_sem=recv.at[b, s],
                device_id=(sp, other),
                device_id_type=MESH,
            )
            copy.start()
            copies.append((b, s, copy))
        own[b] = terms(tp)
    for b in range(BANDS):
        total = own[b]
        for bb, s, copy in copies:
            if bb == b:
                copy.wait()
                total = total + incoming[b, s - 1].astype(F32)
        out_ref[b * half : (b + 1) * half, :] = total.astype(BF16)


def per_device(
    n_sp, n_tp,
    activations, norm_gain, win_query, win_key, win_value, sink_logit, lat_query,
    key_value_down_weight, rope_key, latent_norm_gain, key_up_weight, value_up_weight, out_win, out_lat,
):
    rows, local = activations.shape
    width = local * n_tp
    part = local // SUB
    heads_a = sink_logit.shape[0]
    heads_l = lat_query.shape[1] // (UNROTATED_WIDTH + D_ROPE)
    frequency = 1.0 / ROPE_BASE ** (np.arange(0, D_ROPE, 2) / D_ROPE)
    frequency = np.concatenate([frequency, frequency])[None, :]
    near = np.arange(rows)[:, None] * frequency
    base = (np.arange(n_sp) * rows)[:, None] * frequency
    near = jnp.asarray(np.stack([np.cos(near), np.sin(near)]), F32)
    base = jnp.asarray(np.stack([np.cos(base), np.sin(base)], axis=1), F32)

    vmem = pl.BlockSpec(memory_space=pltpu.VMEM)
    smem = pl.BlockSpec(memory_space=pltpu.SMEM)
    hbm = pl.BlockSpec(memory_space=pl.ANY)
    weights = (key_value_down_weight, rope_key.T, win_key, win_value, win_query, lat_query)
    widths = [w.shape[0] if i == 1 else w.shape[1] for i, w in enumerate(weights)]
    hi = n_sp // 4
    dma = pltpu.SemaphoreType.DMA
    packed = rows + rows // 2
    query, keys, win_out = pl.pallas_call(
        functools.partial(project_kernel, n_sp, n_tp),
        out_shape=(
            jax.ShapeDtypeStruct((heads_l, rows, 2 * UNROTATED_WIDTH), BF16),
            jax.ShapeDtypeStruct((rows * n_sp, 2 * UNROTATED_WIDTH), BF16),
            jax.ShapeDtypeStruct((rows, heads_a * DH), BF16),
        ),
        in_specs=[vmem, vmem, vmem, vmem, smem, vmem, vmem] + [hbm] * 6,
        out_specs=(vmem, vmem, vmem),
        scratch_shapes=[pltpu.VMEM((n_tp * SUB, rows, part), BF16)]
        + [pltpu.VMEM(w.shape, BF16) for w in weights]
        + [pltpu.VMEM((rows, w), F32) for w in widths]
        + [
            pltpu.VMEM((rows, 128), F32),
            pltpu.VMEM((n_sp, packed, UNROTATED_WIDTH), BF16),
            pltpu.VMEM((rows + 2 * WINDOW, 2 * win_key.shape[1]), BF16),
            pltpu.VMEM((rows, win_query.shape[1]), BF16),
            dma((6,)),
            dma((n_tp, SUB)), dma((n_tp, SUB)),
            dma((hi,)), dma((hi,)),
            dma((hi,)), dma((hi,)),
            dma((2 * hi,)), dma((2 * hi,)),
            dma((2,)), dma((2,)),
        ],
        compiler_params=pltpu.CompilerParams(
            collective_id=0, has_side_effects=True, vmem_limit_bytes=56 * 1024 * 1024
        ),
        name="project",
    )(
        activations, norm_gain.reshape(n_tp * SUB, 1, part), near, base, sink_logit,
        latent_norm_gain.reshape(1, -1), key_up_weight, *weights,
    )
    return pl.pallas_call(
        functools.partial(attend_kernel, n_tp),
        out_shape=jax.ShapeDtypeStruct((rows, width // n_tp), BF16),
        in_specs=[vmem, vmem, vmem, vmem, hbm, hbm],
        out_specs=vmem,
        scratch_shapes=[
            pltpu.VMEM(out_win.shape, BF16),
            pltpu.VMEM(out_lat.shape, BF16),
            pltpu.VMEM((heads_l * rows // BANDS, 2 * UNROTATED_WIDTH), F32),
            pltpu.VMEM((heads_l * rows // BANDS, 128), F32),
            pltpu.VMEM((rows // BANDS, heads_l * VALUE_WIDTH), BF16),
            pltpu.VMEM((BANDS, n_tp - 1, rows // BANDS, width // n_tp), BF16),
            pltpu.VMEM((BANDS, n_tp - 1, rows // BANDS, width // n_tp), BF16),
            pltpu.VMEM((BANDS, rows // BANDS, width // n_tp), F32),
            dma((2,)),
            dma((BANDS, n_tp)), dma((BANDS, n_tp)),
        ],
        compiler_params=pltpu.CompilerParams(
            collective_id=1, has_side_effects=True, vmem_limit_bytes=56 * 1024 * 1024
        ),
        name="attend",
    )(query, keys, win_out, value_up_weight, out_win, out_lat)


def solution(mesh):
    return jax.shard_map(
        functools.partial(per_device, mesh.shape["sp"], mesh.shape["tp"]),
        mesh=mesh,
        in_specs=(
            P("sp", "tp"),
            P(),
            P(None, "tp"),
            P(None, "tp"),
            P(None, "tp"),
            P("tp"),
            P(None, "tp"),
            P(),
            P(),
            P(),
            P(None, "tp"),
            P(None, "tp"),
            P("tp", None),
            P("tp", None),
        ),
        out_specs=P("sp", "tp"),
        check_vma=False,
    )
```

profile of v0, /device:TPU:0, one launch (start us, length us, event | category | flops | bytes accessed | tf_op | source)
XLA Modules:
  0.0 61.9 jit_solution(2751759103318415834)
XLA Ops:
  0.0 40.6 %project.1 = (bf16[4,256,256]{2,1,0:T(8,128)(2,1)}, bf16[4096,256]{1,0:T(8,128)(2,1)}, bf16[256,512]{1,0:T(8,128)(2,1)}) custom-call(bf16[256,1024]{1,0:T(8,128)(2,1)} %x_ref.1, f32[4,1,512]{2,1,0:T(1,128)} %bitcast.4, f32[2,256,64]{2,1,0:T(8,128)} %constant.4.clone.near_ref, f32[16,2,64]{2,1,0:T(2,128)} %constant.5.clone.base_ref, f32[8]{0:T(128)} %sink_ref.1, ...), custom_call_target="tpu_custom_call" | custom-call | tf_op jit(solution)/shard_map/project/pallas_call | solution.py:354
  40.7 19.3 %attend.1 = bf16[256,1024]{1,0:T(8,128)(2,1)} custom-call(bf16[4,256,256]{2,1,0:T(8,128)(2,1)} %get-tuple-element.8.q_ref, bf16[4096,256]{1,0:T(8,128)(2,1)} %get-tuple-element.9.kv_ref, bf16[256,512]{1,0:T(8,128)(2,1)} %get-tuple-element.10.win_ref, bf16[128,512]{1,0:T(8,128)(2,1)} %vup_ref.1, bf16[512,2048]{1,0:T(8,128)(2,1)} %ow_hbm.1, ...), custom_call_target="tpu_custom_call" | custom-call | tf_op jit(solution)/shard_map/attend/pallas_call | solution.py:386
  60.0 1.9 %copy.18 = bf16[256,1024]{1,0:T(8,128)(2,1)} copy(bf16[256,1024]{1,0:T(8,128)(2,1)} %attend.1) | data formatting | bytes 1048576
where the time goes:
time: 62.1 us; the launch traced here: 61.9 us
  Pallas kernels  60 us (97%)
  local copies, waits for them, and re-layouts  1.87 us (3%)
    pallas_call x1, Pallas kernels, per_device(): pl.pallas_call(functools.partial(project_kernel, n_sp, n_tp), out_shape=(...  40.6 us
    pallas_call x1, Pallas kernels, per_device(): pl.pallas_call(functools.partial(attend_kernel, n_tp), out_shape=jax.Shap...  19.3 us
    unnamed x1, local copies, waits for them, and re-layouts  1.87 us

commit v1 on v0

v1 whole, which is shorter than its diff:
```python
import functools

import jax
import jax.numpy as jnp
import numpy as np
from jax import lax
from jax.experimental import pallas as pl
from jax.experimental.pallas import tpu as pltpu
from jax.sharding import PartitionSpec as P

HEADS_A = 16
DH = 64
WINDOW = 128
UNROTATED_WIDTH = 128
D_ROPE = 64
VALUE_WIDTH = 128

EPSILON = 1e-06
ROPE_BASE = 10000.0
LOG2E = 1.4426950408889634
MESH = pl.DeviceIdType.MESH
F32 = jnp.float32
BF16 = jnp.bfloat16
LEAD = 32
ONES = 16


def turn(vectors, cosine, sine):
    half = vectors.shape[-1] // 2
    swapped = jnp.concatenate([vectors[:, half:], vectors[:, :half]], axis=1)
    return vectors * cosine + swapped * sine


def dot_nt(a, b):
    return lax.dot_general(a, b, (((1,), (1,)), ((), ())), preferred_element_type=F32)


def dot(a, b):
    return jnp.dot(a, b, preferred_element_type=F32)


def remote(src, dst, send, recv, device):
    return pltpu.make_async_remote_copy(
        src_ref=src, dst_ref=dst, send_sem=send, recv_sem=recv, device_id=device, device_id_type=MESH
    )


def layer_kernel(
    n_sp, n_tp, parts,
    sink_ref,
    x_hbm, gain_hbm, near_hbm, base_hbm, lng_hbm, kup_hbm, vup_hbm,
    wkv_hbm, wr_hbm, wk_hbm, wv_hbm, wq_hbm, wlq_hbm, ow_hbm, ol_hbm,
    own_out, inc_out,
    xv, gain, near, base, lng, kup, vup, wkv, wr, wk, wv, wq, wlq, ow, ol,
    xn, xr, xm, ak, av, aq, alq, akv, ar, scale_ref, cs, ssq_out, ssq_in, pk_out, pk_in,
    gath, latt, qs, qwin, halo, acct, peaks, win, lat, outgoing, own,
    w_sem, x_send, x_recv, s_send, s_recv, p_send, p_recv, z_send, z_recv, y_send, y_recv,
    c_send, c_recv, h_send, h_recv, o_send, o_recv, f_sem,
):
    sp = lax.axis_index("sp")
    tp = lax.axis_index("tp")
    rows, local = xv.shape
    hi = n_sp // 4
    z, y, c = sp // 4, (sp // 2) % 2, sp % 2
    sub = rows // parts
    half = sub // 2
    heads = acct.shape[2] // WINDOW
    k_cols = ak.shape[1]
    cols = own.shape[2]

    def at(zz, yy, cc):
        return (zz * 2 + yy) * 2 + cc

    right, left = (sp + 1) % n_sp, (sp + n_sp - 1) % n_sp
    others = [(s, (tp + s) % n_tp) for s in range(1, n_tp)]
    sources = [(s, (tp + n_tp - s) % n_tp) for s in range(1, n_tp)]

    pairs = (
        (x_hbm, xv), (wkv_hbm, wkv), (wr_hbm, wr), (gain_hbm, gain),
        (near_hbm, near), (base_hbm, base), (lng_hbm, lng),
        (wk_hbm, wk), (wv_hbm, wv), (wq_hbm, wq), (wlq_hbm, wlq),
        (kup_hbm, kup), (vup_hbm, vup), (ow_hbm, ow), (ol_hbm, ol),
    )
    loads = [pltpu.make_async_copy(a, b, w_sem.at[i]) for i, (a, b) in enumerate(pairs)]
    for load in loads[:4]:
        load.start()

    barrier = pltpu.get_barrier_semaphore()
    peers = [(sp, other) for _, other in others]
    peers += [(at((z + d) % hi, y, c), tp) for d in range(1, hi)]
    peers += [(at(z, 1 - y, c), tp), (at(z, y, 1 - c), tp), (right, tp), (left, tp)]
    for peer in peers:
        pl.semaphore_signal(barrier, inc=1, device_id=peer, device_id_type=MESH)
    for load in loads[4:7]:
        load.start()
    latt[UNROTATED_WIDTH:, :] = jnp.ones_like(latt[UNROTATED_WIDTH:, :])
    for load in loads[:4]:
        load.wait()
    for load in loads[7:]:
        load.start()
    pl.semaphore_wait(barrier, len(peers))

    block_at = [(1 - c) * WINDOW, c * WINDOW]
    chunks = [(0, 0, LEAD), (0, LEAD, WINDOW - LEAD), (1, 0, WINDOW)]
    x_copies = {}
    for i, (block, start, size) in enumerate(chunks):
        where = pl.ds(pl.multiple_of(block_at[block] + start, LEAD), size)
        for s, other in others:
            x_copies[s, i] = remote(
                xv.at[where], xr.at[s - 1, where], x_send.at[s, i], x_recv.at[s, i], (sp, other)
            )
    for s, _ in others:
        x_copies[s, 0].start()

    mine = pl.ds(pl.multiple_of(tp * local, local), local)
    wide = xv[...].astype(F32)
    total = jnp.sum(wide * wide, axis=1, keepdims=True)
    ssq_out[...] = jnp.transpose(jnp.broadcast_to(total, (rows, 128)))[0:8]
    xn[...] = (wide * gain[tp]).astype(BF16)
    s_copies = [
        remote(ssq_out, ssq_in.at[s - 1], s_send.at[s], s_recv.at[s], (sp, other)) for s, other in others
    ]
    for copy in s_copies:
        copy.start()
    p_copies = {}
    for g in range(parts):
        span = slice(g * sub, (g + 1) * sub)
        comp = dot(xn[span], wkv[mine, :])
        turned = dot_nt(xn[span], wr[:, mine])
        akv[span] = comp
        ar[span] = turned
        pk_out[g, 0:sub] = comp.astype(BF16)
        pk_out[g, sub:] = jnp.concatenate([turned[:half], turned[half:]], axis=1).astype(BF16)
        for s, other in others:
            p_copies[s, g] = remote(
                pk_out.at[g], pk_in.at[s - 1, g], p_send.at[s, g], p_recv.at[s, g], (sp, other)
            )
            p_copies[s, g].start()
    for i in range(1, len(chunks)):
        for s, _ in others:
            x_copies[s, i].start()

    for load in loads[4:7]:
        load.wait()
    near_cos, near_sin = near[0], near[1]
    base_cos, base_sin = base[sp, 0:1, :], base[sp, 1:2, :]
    plain_sine = near_sin * base_cos + near_cos * base_sin
    lane = lax.broadcasted_iota(jnp.int32, plain_sine.shape, 1)
    cs[0] = near_cos * base_cos - near_sin * base_sin
    cs[1] = jnp.where(lane < D_ROPE // 2, -plain_sine, plain_sine)

    big = ((wk, ak), (wv, av), (wq, aq), (wlq, alq))
    for load, (weight, acc) in zip(loads[7:11], big):
        load.wait()
        acc[...] = dot(xn[...], weight[mine, :])

    relayed = hi == 4
    inner = (z + 1) % 4 >= 2
    if relayed:
        far = 2 - z // 2
        z_of = [z, z + 1 - 2 * (z % 2), far, 3 * (1 - z // 2)]
        z_to = {1: z_of[1], 2: far}
    else:
        z_of = [(z + hi - d) % hi for d in range(hi)]
        z_to = {d: (z + d) % hi for d in range(1, hi)}
    to_y, to_c = (at(z, 1 - y, c), tp), (at(z, y, 1 - c), tp)
    sends = []

    def forward(block, g, send, recv, device):
        copy = remote(gath.at[block, g], gath.at[block, g], send, recv, device)
        copy.start()
        return copy

    def block_of(d, dy, dc):
        return at(z_of[d], 1 - y if dy else y, 1 - c if dc else c)

    def to_core(d, dy, g):
        k = d + hi * dy
        sends.append(forward(block_of(d, dy, 0), g, c_send.at[k, g], c_recv.at[k, g], to_c))

    def to_row(d, g):
        sends.append(forward(block_of(d, 0, 0), g, y_send.at[d, g], y_recv.at[d, g], to_y))

    relays = []

    def got_z(d, g):
        block = block_of(d, 0, 0)
        origin = z_of[d]
        remote(
            gath.at[block, g], gath.at[block, g], z_send.at[d, g], z_recv.at[origin, g], to_y
        ).wait_recv()
        if relayed and d >= 2:
            copy = remote(
                gath.at[block, g], gath.at[block, g], z_send.at[(0, 3)[d - 2], g], z_recv.at[origin, g],
                (at(z_of[1], y, c), tp),
            )
            relays.append(copy)

            @pl.when(inner)
            def _():
                copy.start()
        to_row(d, g)
        to_core(d, 0, g)

    def got_y(d, g):
        block = block_of(d, 1, 0)
        remote(gath.at[block, g], gath.at[block, g], y_send.at[d, g], y_recv.at[d, g], to_y).wait_recv()
        to_core(d, 1, g)

    def got_c(d):
        for dy in range(2):
            for g in range(parts):
                block, k = block_of(d, dy, 1), d + hi * dy
                remote(gath.at[block, g], gath.at[block, g], c_send.at[k, g], c_recv.at[k, g], to_c).wait_recv()

    for copy in s_copies:
        copy.wait_recv()
    total = ssq_out[...]
    for s, _ in sources:
        total = total + ssq_in[s - 1]
    factor = lax.rsqrt(total / (local * n_tp) + EPSILON)
    scale_ref[...] = jnp.transpose(jnp.broadcast_to(factor[0:1], (128, rows)))
    for g in range(parts):
        span = slice(g * sub, (g + 1) * sub)
        comp = akv[span]
        turned = ar[span]
        for s, _ in sources:
            p_copies[s, g].wait_recv()
            comp = comp + pk_in[s - 1, g, 0:sub].astype(F32)
            both = pk_in[s - 1, g, sub:].astype(F32)
            turned = turned + jnp.concatenate([both[:, :D_ROPE], both[:, D_ROPE:]], axis=0)
        latent = comp * lax.rsqrt(jnp.mean(comp * comp, axis=1, keepdims=True) + EPSILON) * lng[...]
        turned = turn(turned * scale_ref[span, 0:D_ROPE], cs[0, span], cs[1, span])
        gath[sp, g, 0:sub] = latent.astype(BF16)
        gath[sp, g, sub:] = jnp.concatenate([turned[:half], turned[half:]], axis=1).astype(BF16)
        for d, zz in z_to.items():
            sends.append(forward(sp, g, z_send.at[d, g], z_recv.at[z, g], (at(zz, y, c), tp)))
        to_row(0, g)
        to_core(0, 0, g)

    def widen(scale, width):
        return jnp.concatenate([scale] * (-(-width // 128)), axis=1)[:, :width]

    def arrive(index):
        for i, (block, _, _) in enumerate(chunks):
            if block == index:
                for s, _ in others:
                    x_copies[s, i].wait_recv()
        where = pl.ds(pl.multiple_of(block_at[index], WINDOW), WINDOW)
        for s, source in sources:
            xm[s - 1] = (xr[s - 1, where, :].astype(F32) * gain[source]).astype(BF16)

    def finish(index, weight, acc):
        where = pl.ds(pl.multiple_of(block_at[index], WINDOW), WINDOW)
        result = acc[where, :]
        for s, source in sources:
            theirs = pl.ds(pl.multiple_of(source * local, local), local)
            result = result + dot(xm[s - 1], weight[theirs, :])
        return result * widen(scale_ref[where, :], result.shape[1])

    h_copies = []

    def keys_values(index):
        where = pl.ds(pl.multiple_of(WINDOW + block_at[index], WINDOW), WINDOW)
        halo[where, 0:k_cols] = finish(index, wk, ak).astype(BF16)
        halo[where, k_cols:] = finish(index, wv, av).astype(BF16)
        if index == 0:
            target, spot = at(z, y, 1 - c), c * (rows + WINDOW)
        else:
            target, spot = (sp + n_sp + 2 * c - 1) % n_sp, (1 - c) * (rows + WINDOW)
        copy = remote(
            halo.at[where],
            halo.at[pl.ds(pl.multiple_of(spot, WINDOW), WINDOW)],
            h_send.at[index], h_recv.at[index], (target, tp),
        )
        copy.start()
        h_copies.append(copy)

    per_head = UNROTATED_WIDTH + D_ROPE
    softmax = per_head ** (-0.5) * LOG2E

    def queries(index):
        where = pl.ds(pl.multiple_of(block_at[index], WINDOW), WINDOW)
        qwin[index] = finish(index, wq, aq).astype(BF16)
        every = finish(index, wlq, alq)
        cosine, sine = cs[0, where, :], cs[1, where, :]
        for h in range(heads):
            one = every[:, h * per_head : (h + 1) * per_head]
            plain = one[:, :UNROTATED_WIDTH].astype(BF16)
            seen = (dot_nt(plain, kup[:, h * UNROTATED_WIDTH : (h + 1) * UNROTATED_WIDTH]) * softmax).astype(BF16)
            turned = turn(one[:, UNROTATED_WIDTH:], cosine, sine) * softmax
            zero = jnp.zeros_like(turned)
            at_rows = slice(h * WINDOW, (h + 1) * WINDOW)
            for v, packed in enumerate(((turned, zero), (zero, turned))):
                qs[v, index, at_rows, 0:UNROTATED_WIDTH] = seen
                qs[v, index, at_rows, UNROTATED_WIDTH:] = jnp.concatenate(packed, axis=1).astype(BF16)

    eye = jnp.where(
        lax.broadcasted_iota(jnp.int32, (UNROTATED_WIDTH, UNROTATED_WIDTH), 0)
        == lax.broadcasted_iota(jnp.int32, (UNROTATED_WIDTH, UNROTATED_WIDTH), 1),
        1.0,
        0.0,
    ).astype(BF16)
    chunk = 4 * rows

    def pieces(d):
        return [(block_of(d, dy, dc), g) for dc in range(2) for dy in range(2) for g in range(parts)]

    def ready(d):
        got_c(d)
        for v in range(2):
            latents = jnp.concatenate(
                [gath[block, g, v * half : (v + 1) * half, :] for block, g in pieces(d)], axis=0
            )
            start = d * chunk + v * (chunk // 2)
            latt[0:UNROTATED_WIDTH, start : start + chunk // 2] = dot_nt(eye, latents).astype(BF16)

    def attend(index, d):
        scores = []
        for v in range(2):
            keys = jnp.concatenate(
                [
                    jnp.concatenate(
                        [gath[block, g, v * half : (v + 1) * half, :], gath[block, g, sub : sub + half, :]], axis=1
                    )
                    for block, g in pieces(d)
                ],
                axis=0,
            )
            scores.append(dot_nt(keys, qs[v, index]))
        new = jnp.maximum(jnp.max(scores[0], axis=0, keepdims=True), jnp.max(scores[1], axis=0, keepdims=True))
        if d > 0:
            old = peaks[index, 0:1]
            new = jnp.maximum(old, new)
        weight = jnp.concatenate([jnp.exp2(part - new).astype(BF16) for part in scores], axis=0)
        added = dot(latt[:, d * chunk : (d + 1) * chunk], weight)
        acct[index] = added if d == 0 else acct[index] * jnp.exp2(old - new) + added
        peaks[index] = jnp.broadcast_to(new, peaks.shape[1:])

    reach = 3 * WINDOW
    seq_total = rows * n_sp

    def window(index):
        start = block_at[index]
        spots = lax.broadcasted_iota(jnp.int32, (WINDOW, reach), 0)
        keys_at = lax.broadcasted_iota(jnp.int32, (WINDOW, reach), 1)
        distance = jnp.abs(spots + WINDOW - keys_at)
        key_pos = sp * rows + start - WINDOW + keys_at
        inside = (distance <= WINDOW) & (key_pos >= 0) & (key_pos < seq_total)
        gone = jnp.where(inside, distance.astype(F32), jnp.inf)
        where = pl.ds(pl.multiple_of(start, WINDOW), reach)
        group = 2
        for kv_head in range(k_cols // DH):
            keys = halo[where, kv_head * DH : (kv_head + 1) * DH]
            values = halo[where, k_cols + kv_head * DH : k_cols + (kv_head + 1) * DH]
            first = kv_head * group
            query = jnp.concatenate(
                [qwin[index, :, (first + j) * DH : (first + j + 1) * DH] for j in range(group)], axis=0
            )
            dots = dot_nt(query, keys) * (DH ** (-0.5) * LOG2E)
            weights, bottoms = [], []
            for j in range(group):
                head = first + j
                place = (tp * sink_ref.shape[0] + head + 1).astype(F32)
                slope = jnp.exp2(jnp.full((1, reach), -8.0 / HEADS_A, F32) * place) * LOG2E
                sink = sink_ref[head] * LOG2E
                scores = dots[j * WINDOW : (j + 1) * WINDOW] - slope * gone
                peak = jnp.maximum(jnp.max(scores, axis=1, keepdims=True), sink)
                weight = jnp.exp2(scores - peak)
                bottoms.append(jnp.sum(weight, axis=1, keepdims=True) + jnp.exp2(sink - peak))
                weights.append(weight.astype(BF16))
            blended = dot(jnp.concatenate(weights, axis=0), values)
            outs = [blended[j * WINDOW : (j + 1) * WINDOW] / bottoms[j] for j in range(group)]
            win[index, :, first * DH : (first + group) * DH] = jnp.concatenate(outs, axis=1).astype(BF16)

    o_copies, f_copies = [], []

    def give(index):
        inverse = 1.0 / acct[index, UNROTATED_WIDTH : UNROTATED_WIDTH + 1, :]
        for h in range(heads):
            where = slice(h * WINDOW, (h + 1) * WINDOW)
            blended = jnp.transpose(acct[index, 0:UNROTATED_WIDTH, where] * inverse[:, where]).astype(BF16)
            spot = slice(h * VALUE_WIDTH, (h + 1) * VALUE_WIDTH)
            lat[index, :, spot] = dot(blended, vup[:, spot]).astype(BF16)

        def terms(j):
            where = pl.ds(pl.multiple_of(j * cols, cols), cols)
            return dot(win[index], ow[:, where]) + dot(lat[index], ol[:, where])

        where = pl.ds(pl.multiple_of(block_at[index], WINDOW), WINDOW)
        for s, other in others:
            outgoing[index, s - 1] = terms(other).astype(BF16)
            copy = remote(
                outgoing.at[index, s - 1], inc_out.at[s - 1, where], o_send.at[index, s], o_recv.at[index, s],
                (sp, other),
            )
            copy.start()
            o_copies.append(copy)
        own[index] = terms(tp)
        copy = pltpu.make_async_copy(own.at[index], own_out.at[where], f_sem.at[index])
        copy.start()
        f_copies.append(copy)

    both = range(parts)
    for g in both:
        got_y(0, g)
        if hi > 1:
            got_z(1, g)
    arrive(0)
    keys_values(0)
    for load in loads[11:]:
        load.wait()
    queries(0)
    ready(0)
    if relayed:
        for g in both:
            got_z(2, g)
        attend(0, 0)
        for g in both:
            got_y(1, g)
            got_z(3, g)
        ready(1)
        attend(0, 1)
        arrive(1)
        keys_values(1)
        for g in both:
            got_y(2, g)
        h_copies[0].wait_recv()
        window(0)
        for g in both:
            got_y(3, g)
        ready(2)
        attend(0, 2)
        ready(3)
        attend(0, 3)
    else:
        attend(0, 0)
        for d in range(1, hi):
            for g in both:
                got_y(d, g)
                if d + 1 < hi:
                    got_z(d + 1, g)
            ready(d)
            attend(0, d)
        arrive(1)
        keys_values(1)
        h_copies[0].wait_recv()
        window(0)
    give(0)
    queries(1)
    for d in range(hi):
        attend(1, d)
    h_copies[1].wait_recv()
    window(1)
    give(1)

    for copy in list(x_copies.values()) + s_copies + list(p_copies.values()) + sends + h_copies:
        copy.wait_send()
    if relayed:

        @pl.when(inner)
        def _():
            for copy in relays:
                copy.wait_send()

    for copy in f_copies + o_copies:
        copy.wait()


def per_device(
    n_sp, n_tp,
    activations, norm_gain, win_query, win_key, win_value, sink_logit, lat_query,
    key_value_down_weight, rope_key, latent_norm_gain, key_up_weight, value_up_weight, out_win, out_lat,
):
    rows, local = activations.shape
    width = local * n_tp
    cols = width // n_tp
    parts = 2
    heads_a = sink_logit.shape[0]
    heads_l = lat_query.shape[1] // (UNROTATED_WIDTH + D_ROPE)
    frequency = 1.0 / ROPE_BASE ** (np.arange(0, D_ROPE, 2) / D_ROPE)
    frequency = np.concatenate([frequency, frequency])[None, :]
    near = np.arange(rows)[:, None] * frequency
    base = (np.arange(n_sp) * rows)[:, None] * frequency
    near = jnp.asarray(np.stack([np.cos(near), np.sin(near)]), F32)
    base = jnp.asarray(np.stack([np.cos(base), np.sin(base)], axis=1), F32)

    smem = pl.BlockSpec(memory_space=pltpu.SMEM)
    hbm = pl.BlockSpec(memory_space=pl.ANY)
    dma = pltpu.SemaphoreType.DMA
    operands = (
        activations, norm_gain.reshape(n_tp, 1, local), near, base, latent_norm_gain.reshape(1, -1),
        key_up_weight, value_up_weight,
        key_value_down_weight, rope_key.T, win_key, win_value, win_query, lat_query, out_win, out_lat,
    )
    order = (0, 1, 2, 3, 4, 5, 6, 7, 8, 9, 10, 11, 12, 13, 14)
    hi = n_sp // 4
    sub = rows // parts
    packed = sub + sub // 2
    blocks = rows // WINDOW
    span = heads_l * WINDOW

    def vmem(shape, kind=BF16):
        return pltpu.VMEM(shape, kind)

    own, incoming = pl.pallas_call(
        functools.partial(layer_kernel, n_sp, n_tp, parts),
        out_shape=(
            jax.ShapeDtypeStruct((rows, cols), F32),
            jax.ShapeDtypeStruct((n_tp - 1, rows, cols), BF16),
        ),
        in_specs=[smem] + [hbm] * len(operands),
        out_specs=(hbm, hbm),
        scratch_shapes=[vmem(operands[i].shape, operands[i].dtype) for i in order]
        + [
            vmem((rows, local)),
            vmem((n_tp - 1, rows, local)),
            vmem((n_tp - 1, WINDOW, local)),
            vmem((rows, win_key.shape[1]), F32),
            vmem((rows, win_value.shape[1]), F32),
            vmem((rows, win_query.shape[1]), F32),
            vmem((rows, lat_query.shape[1]), F32),
            vmem((rows, UNROTATED_WIDTH), F32),
            vmem((rows, D_ROPE), F32),
            vmem((rows, 128), F32),
            vmem((2, rows, D_ROPE), F32),
            vmem((8, rows), F32),
            vmem((n_tp - 1, 8, rows), F32),
            vmem((parts, packed, UNROTATED_WIDTH)),
            vmem((n_tp - 1, parts, packed, UNROTATED_WIDTH)),
            vmem((n_sp, parts, packed, UNROTATED_WIDTH)),
            vmem((UNROTATED_WIDTH + ONES, rows * n_sp)),
            vmem((2, blocks, span, 2 * UNROTATED_WIDTH)),
            vmem((blocks, WINDOW, win_query.shape[1])),
            vmem((rows + 2 * WINDOW, 2 * win_key.shape[1])),
            vmem((blocks, UNROTATED_WIDTH + ONES, span), F32),
            vmem((blocks, 8, span), F32),
            vmem((blocks, WINDOW, heads_a * DH)),
            vmem((blocks, WINDOW, heads_l * VALUE_WIDTH)),
            vmem((blocks, n_tp - 1, WINDOW, cols)),
            vmem((blocks, WINDOW, cols), F32),
            dma((len(operands),)),
            dma((n_tp, 3)), dma((n_tp, 3)),
            dma((n_tp,)), dma((n_tp,)),
            dma((n_tp, parts)), dma((n_tp, parts)),
            dma((hi, parts)), dma((hi, parts)),
            dma((hi, parts)), dma((hi, parts)),
            dma((2 * hi, parts)), dma((2 * hi, parts)),
            dma((2,)), dma((2,)),
            dma((blocks, n_tp)), dma((blocks, n_tp)),
            dma((blocks,)),
        ],
        compiler_params=pltpu.CompilerParams(
            collective_id=0, has_side_effects=True, vmem_limit_bytes=60 * 1024 * 1024
        ),
        name="layer",
    )(sink_logit, *operands)
    total = own
    for s in range(n_tp - 1):
        total = total + incoming[s].astype(F32)
    return total.astype(BF16)


def solution(mesh):
    return jax.shard_map(
        functools.partial(per_device, mesh.shape["sp"], mesh.shape["tp"]),
        mesh=mesh,
        in_specs=(
            P("sp", "tp"),
            P(),
            P(None, "tp"),
            P(None, "tp"),
            P(None, "tp"),
            P("tp"),
            P(None, "tp"),
            P(),
            P(),
            P(),
            P(None, "tp"),
            P(None, "tp"),
            P("tp", None),
            P("tp", None),
        ),
        out_specs=P("sp", "tp"),
        check_vma=False,
    )
```

time: 62.1 us -> 48.9 us (0.79)
  Pallas kernels: 60 us -> 46.4 us
  other arithmetic: 0 us -> 2.3 us
  local copies, waits for them, and re-layouts: 1.87 us -> 0 us
    pallas_call x2 -> x1, Pallas kernels: 60 us -> 46.4 us  [per_device(): pl.pallas_call(functools.partial(layer_kernel, n_sp, n_tp, parts), out_sh...]
    convert_element_type x0 -> x1, other arithmetic: none -> 2.3 us  [per_device(): return total.astype(BF16)]
    unnamed x1 -> x0, local copies, waits for them, and re-layouts: 1.87 us -> none
where the time goes in v1:
time: 48.9 us; the launch traced here: 48.7 us
  Pallas kernels  46.4 us (95%)
  other arithmetic  2.3 us (5%)
    pallas_call x1, Pallas kernels, per_device(): pl.pallas_call(functools.partial(layer_kernel, n_sp, n_tp, parts), out_sh...  46.4 us
    convert_element_type x1, other arithmetic, per_device(): return total.astype(BF16)  2.3 us

profile of v1, /device:TPU:0, one launch (start us, length us, event | category | flops | bytes accessed | tf_op | source)
XLA Modules:
  0.0 48.7 jit_solution(8719629335234385711)
XLA Ops:
  0.0 46.4 %layer.1 = (f32[256,1024]{1,0:T(8,128)}, bf16[1,256,1024]{2,1,0:T(8,128)(2,1)}) custom-call(f32[8]{0:T(128)} %sink_ref.1, bf16[256,1024]{1,0:T(8,128)(2,1)} %x_hbm.1, f32[2,1,1024]{2,1,0:T(1,128)} %bitcast.7, f32[2,256,64]{2,1,0:T(8,128)} %constant.4.clone.near_hbm, f32[16,2,64]{2,1,0:T(2,128)} %constant.5.clone.base_hbm, f32[1,128]{1,0:T(1,128)} %bitcast.8, ...), custom_call_target="tpu_custom_call" | custom-call | tf_op jit(solution)/shard_map/layer/pallas_call | solution.py:506
  46.4 2.3 %fusion = bf16[256,1024]{1,0:T(8,128)(2,1)} fusion(f32[256,1024]{1,0:T(8,128)} %get-tuple-element.7, bf16[1,256,1024]{2,1,0:T(8,128)(2,1)} %get-tuple-element.8), kind=kLoop, calls=%fused_computation.1 | loop fusion | flops 786432 | bytes 2097152 | tf_op jit(solution)/shard_map/convert_element_type | solution.py:561

commit v2 on v1

--- a/solution.py
+++ b/solution.py
@@ -21,7 +21,6 @@
 MESH = pl.DeviceIdType.MESH
 F32 = jnp.float32
 BF16 = jnp.bfloat16
-LEAD = 32
 ONES = 16
 
 
@@ -53,9 +52,9 @@
     own_out, inc_out,
     xv, gain, near, base, lng, kup, vup, wkv, wr, wk, wv, wq, wlq, ow, ol,
     xn, xr, xm, ak, av, aq, alq, akv, ar, scale_ref, cs, ssq_out, ssq_in, pk_out, pk_in,
-    gath, latt, qs, qwin, halo, acct, peaks, win, lat, outgoing, own,
+    gath, latt, qs, qwin, halo, vt, acct, peaks, win, outgoing, own,
     w_sem, x_send, x_recv, s_send, s_recv, p_send, p_recv, z_send, z_recv, y_send, y_recv,
-    c_send, c_recv, h_send, h_recv, o_send, o_recv, f_sem,
+    c_send, c_recv, h_send, h_recv, o_send, o_recv, f_sem, gate,
 ):
     sp = lax.axis_index("sp")
     tp = lax.axis_index("tp")
@@ -71,7 +70,6 @@
     def at(zz, yy, cc):
         return (zz * 2 + yy) * 2 + cc
 
-    right, left = (sp + 1) % n_sp, (sp + n_sp - 1) % n_sp
     others = [(s, (tp + s) % n_tp) for s in range(1, n_tp)]
     sources = [(s, (tp + n_tp - s) % n_tp) for s in range(1, n_tp)]
 
@@ -86,11 +84,32 @@
         load.start()
 
     barrier = pltpu.get_barrier_semaphore()
-    peers = [(sp, other) for _, other in others]
-    peers += [(at((z + d) % hi, y, c), tp) for d in range(1, hi)]
-    peers += [(at(z, 1 - y, c), tp), (at(z, y, 1 - c), tp), (right, tp), (left, tp)]
-    for peer in peers:
-        pl.semaphore_signal(barrier, inc=1, device_id=peer, device_id_type=MESH)
+    late = (sp + n_sp + 2 * c - 1) % n_sp
+    across = y == c
+
+    def rank(zz):
+        return (zz > 0).astype(jnp.int32) + ((zz > 0) & (zz < hi - 1)).astype(jnp.int32)
+
+    distant = [(None, (z + d) % hi, at((z + d) % hi, y, c)) for d in range(1, hi)]
+    distant.append((across, late // 4, late))
+    expected, gated, gates = n_tp + 1, 0, []
+    for _, other in others:
+        pl.semaphore_signal(barrier, inc=1, device_id=(sp, other), device_id_type=MESH)
+    for peer in (at(z, 1 - y, c), at(z, y, 1 - c)):
+        pl.semaphore_signal(barrier, inc=1, device_id=(peer, tp), device_id_type=MESH)
+    for only, zz, peer in distant:
+        first, same = rank(z) < rank(zz), rank(z) == rank(zz)
+        if only is not None:
+            first, same = first & only, same | jnp.logical_not(only)
+        last_in = jnp.logical_not(first | same)
+        expected = expected + (last_in | same).astype(jnp.int32)
+        gated = gated + first.astype(jnp.int32)
+        gates.append((last_in, peer))
+
+        @pl.when(first | same)
+        def _():
+            pl.semaphore_signal(barrier, inc=1, device_id=(peer, tp), device_id_type=MESH)
+
     for load in loads[4:7]:
         load.start()
     latt[UNROTATED_WIDTH:, :] = jnp.ones_like(latt[UNROTATED_WIDTH:, :])
@@ -98,31 +117,11 @@
         load.wait()
     for load in loads[7:]:
         load.start()
-    pl.semaphore_wait(barrier, len(peers))
-
-    block_at = [(1 - c) * WINDOW, c * WINDOW]
-    chunks = [(0, 0, LEAD), (0, LEAD, WINDOW - LEAD), (1, 0, WINDOW)]
-    x_copies = {}
-    for i, (block, start, size) in enumerate(chunks):
-        where = pl.ds(pl.multiple_of(block_at[block] + start, LEAD), size)
-        for s, other in others:
-            x_copies[s, i] = remote(
-                xv.at[where], xr.at[s - 1, where], x_send.at[s, i], x_recv.at[s, i], (sp, other)
-            )
-    for s, _ in others:
-        x_copies[s, 0].start()
-
     mine = pl.ds(pl.multiple_of(tp * local, local), local)
     wide = xv[...].astype(F32)
     total = jnp.sum(wide * wide, axis=1, keepdims=True)
     ssq_out[...] = jnp.transpose(jnp.broadcast_to(total, (rows, 128)))[0:8]
     xn[...] = (wide * gain[tp]).astype(BF16)
-    s_copies = [
-        remote(ssq_out, ssq_in.at[s - 1], s_send.at[s], s_recv.at[s], (sp, other)) for s, other in others
-    ]
-    for copy in s_copies:
-        copy.start()
-    p_copies = {}
     for g in range(parts):
         span = slice(g * sub, (g + 1) * sub)
         comp = dot(xn[span], wkv[mine, :])
@@ -131,13 +130,35 @@
         ar[span] = turned
         pk_out[g, 0:sub] = comp.astype(BF16)
         pk_out[g, sub:] = jnp.concatenate([turned[:half], turned[half:]], axis=1).astype(BF16)
+
+    pl.semaphore_wait(barrier, expected)
+    for last_in, peer in gates:
+
+        @pl.when(last_in)
+        def _():
+            pl.semaphore_signal(gate, inc=1, device_id=(peer, tp), device_id_type=MESH)
+
+    s_copies = [
+        remote(ssq_out, ssq_in.at[s - 1], s_send.at[s], s_recv.at[s], (sp, other)) for s, other in others
+    ]
+    for copy in s_copies:
+        copy.start()
+    p_copies = {}
+    for g in range(parts):
         for s, other in others:
             p_copies[s, g] = remote(
                 pk_out.at[g], pk_in.at[s - 1, g], p_send.at[s, g], p_recv.at[s, g], (sp, other)
             )
             p_copies[s, g].start()
-    for i in range(1, len(chunks)):
-        for s, _ in others:
+
+    block_at = [(1 - c) * WINDOW, c * WINDOW]
+    x_copies = {}
+    for i in range(2):
+        where = pl.ds(pl.multiple_of(block_at[i], WINDOW), WINDOW)
+        for s, other in others:
+            x_copies[s, i] = remote(
+                xv.at[where], xr.at[s - 1, where], x_send.at[s, i], x_recv.at[s, i], (sp, other)
+            )
             x_copies[s, i].start()
 
     for load in loads[4:7]:
@@ -164,57 +185,69 @@
         z_of = [(z + hi - d) % hi for d in range(hi)]
         z_to = {d: (z + d) % hi for d in range(1, hi)}
     to_y, to_c = (at(z, 1 - y, c), tp), (at(z, y, 1 - c), tp)
-    sends = []
-
-    def forward(block, g, send, recv, device):
-        copy = remote(gath.at[block, g], gath.at[block, g], send, recv, device)
-        copy.start()
-        return copy
+    sent = {}
 
     def block_of(d, dy, dc):
         return at(z_of[d], 1 - y if dy else y, 1 - c if dc else c)
 
+    def own_to_z(d, g):
+        part = gath.at[sp, g]
+        return remote(part, part, z_send.at[d, g], z_recv.at[z, g], (at(z_to[d], y, c), tp))
+
+    def from_z(d, g):
+        part = gath.at[block_of(d, 0, 0), g]
+        return remote(part, part, z_send.at[d, g], z_recv.at[z_of[d], g], to_y)
+
+    def relay(d, g):
+        part = gath.at[block_of(d, 0, 0), g]
+        return remote(part, part, z_send.at[(0, 3)[d - 2], g], z_recv.at[z_of[d], g], (at(z_of[1], y, c), tp))
+
+    def to_row(d, g):
+        part = gath.at[block_of(d, 0, 0), g]
+        return remote(part, part, y_send.at[d, g], y_recv.at[d, g], to_y)
+
+    def from_row(d, g):
+        part = gath.at[block_of(d, 1, 0), g]
+        return remote(part, part, y_send.at[d, g], y_recv.at[d, g], to_y)
+
     def to_core(d, dy, g):
-        k = d + hi * dy
-        sends.append(forward(block_of(d, dy, 0), g, c_send.at[k, g], c_recv.at[k, g], to_c))
-
-    def to_row(d, g):
-        sends.append(forward(block_of(d, 0, 0), g, y_send.at[d, g], y_recv.at[d, g], to_y))
-
-    relays = []
-
-    def got_z(d, g):
-        block = block_of(d, 0, 0)
-        origin = z_of[d]
-        remote(
-            gath.at[block, g], gath.at[block, g], z_send.at[d, g], z_recv.at[origin, g], to_y
-        ).wait_recv()
+        part, k = gath.at[block_of(d, dy, 0), g], d + hi * dy
+        return remote(part, part, c_send.at[k, g], c_recv.at[k, g], to_c)
+
+    def from_core(d, dy, g):
+        part, k = gath.at[block_of(d, dy, 1), g], d + hi * dy
+        return remote(part, part, c_send.at[k, g], c_recv.at[k, g], to_c)
+
+    def start(make, *spot):
+        make(*spot).start()
+        sent[(make, *spot)] = functools.partial(make, *spot)
+
+    def got_z(d, g, role=None):
+        from_z(d, g).wait_recv()
         if relayed and d >= 2:
-            copy = remote(
-                gath.at[block, g], gath.at[block, g], z_send.at[(0, 3)[d - 2], g], z_recv.at[origin, g],
-                (at(z_of[1], y, c), tp),
-            )
-            relays.append(copy)
-
-            @pl.when(inner)
-            def _():
-                copy.start()
-        to_row(d, g)
-        to_core(d, 0, g)
+            if role is None:
+                pl.when(inner)(relay(d, g).start)
+            elif role:
+                relay(d, g).start()
+        start(to_row, d, g)
+        start(to_core, d, 0, g)
 
     def got_y(d, g):
-        block = block_of(d, 1, 0)
-        remote(gath.at[block, g], gath.at[block, g], y_send.at[d, g], y_recv.at[d, g], to_y).wait_recv()
-        to_core(d, 1, g)
+        from_row(d, g).wait_recv()
+        start(to_core, d, 1, g)
 
     def got_c(d):
         for dy in range(2):
             for g in range(parts):
-                block, k = block_of(d, dy, 1), d + hi * dy
-                remote(gath.at[block, g], gath.at[block, g], c_send.at[k, g], c_recv.at[k, g], to_c).wait_recv()
+                from_core(d, dy, g).wait_recv()
 
     for copy in s_copies:
         copy.wait_recv()
+
+    @pl.when(gated > 0)
+    def _():
+        pl.semaphore_wait(gate, gated)
+
     total = ssq_out[...]
     for s, _ in sources:
         total = total + ssq_in[s - 1]
@@ -233,19 +266,17 @@
         turned = turn(turned * scale_ref[span, 0:D_ROPE], cs[0, span], cs[1, span])
         gath[sp, g, 0:sub] = latent.astype(BF16)
         gath[sp, g, sub:] = jnp.concatenate([turned[:half], turned[half:]], axis=1).astype(BF16)
-        for d, zz in z_to.items():
-            sends.append(forward(sp, g, z_send.at[d, g], z_recv.at[z, g], (at(zz, y, c), tp)))
-        to_row(0, g)
-        to_core(0, 0, g)
+        for d in reversed(z_to):
+            start(own_to_z, d, g)
+        start(to_row, 0, g)
+        start(to_core, 0, 0, g)
 
     def widen(scale, width):
         return jnp.concatenate([scale] * (-(-width // 128)), axis=1)[:, :width]
 
     def arrive(index):
-        for i, (block, _, _) in enumerate(chunks):
-            if block == index:
-                for s, _ in others:
-                    x_copies[s, i].wait_recv()
+        for s, _ in others:
+            x_copies[s, index].wait_recv()
         where = pl.ds(pl.multiple_of(block_at[index], WINDOW), WINDOW)
         for s, source in sources:
             xm[s - 1] = (xr[s - 1, where, :].astype(F32) * gain[source]).astype(BF16)
@@ -267,7 +298,7 @@
         if index == 0:
             target, spot = at(z, y, 1 - c), c * (rows + WINDOW)
         else:
-            target, spot = (sp + n_sp + 2 * c - 1) % n_sp, (1 - c) * (rows + WINDOW)
+            target, spot = late, (1 - c) * (rows + WINDOW)
         copy = remote(
             halo.at[where],
             halo.at[pl.ds(pl.multiple_of(spot, WINDOW), WINDOW)],
@@ -275,6 +306,7 @@
         )
         copy.start()
         h_copies.append(copy)
+        flip(WINDOW + block_at[index])
 
     per_head = UNROTATED_WIDTH + D_ROPE
     softmax = per_head ** (-0.5) * LOG2E
@@ -284,15 +316,18 @@
         qwin[index] = finish(index, wq, aq).astype(BF16)
         every = finish(index, wlq, alq)
         cosine, sine = cs[0, where, :], cs[1, where, :]
+        ones_of = [every[:, h * per_head : (h + 1) * per_head] for h in range(heads)]
+        seen = [
+            dot_nt(ones_of[h][:, :UNROTATED_WIDTH].astype(BF16), kup[:, h * UNROTATED_WIDTH : (h + 1) * UNROTATED_WIDTH])
+            for h in range(heads)
+        ]
         for h in range(heads):
-            one = every[:, h * per_head : (h + 1) * per_head]
-            plain = one[:, :UNROTATED_WIDTH].astype(BF16)
-            seen = (dot_nt(plain, kup[:, h * UNROTATED_WIDTH : (h + 1) * UNROTATED_WIDTH]) * softmax).astype(BF16)
-            turned = turn(one[:, UNROTATED_WIDTH:], cosine, sine) * softmax
+            turned = turn(ones_of[h][:, UNROTATED_WIDTH:], cosine, sine) * softmax
             zero = jnp.zeros_like(turned)
             at_rows = slice(h * WINDOW, (h + 1) * WINDOW)
+            plain = (seen[h] * softmax).astype(BF16)
             for v, packed in enumerate(((turned, zero), (zero, turned))):
-                qs[v, index, at_rows, 0:UNROTATED_WIDTH] = seen
+                qs[v, index, at_rows, 0:UNROTATED_WIDTH] = plain
                 qs[v, index, at_rows, UNROTATED_WIDTH:] = jnp.concatenate(packed, axis=1).astype(BF16)
 
     eye = jnp.where(
@@ -315,8 +350,10 @@
             start = d * chunk + v * (chunk // 2)
             latt[0:UNROTATED_WIDTH, start : start + chunk // 2] = dot_nt(eye, latents).astype(BF16)
 
-    def attend(index, d):
-        scores = []
+    tile = min(2 * WINDOW, heads * WINDOW)
+
+    def scores_of(index, d, t):
+        found = []
         for v in range(2):
             keys = jnp.concatenate(
                 [
@@ -327,65 +364,110 @@
                 ],
                 axis=0,
             )
-            scores.append(dot_nt(keys, qs[v, index]))
-        new = jnp.maximum(jnp.max(scores[0], axis=0, keepdims=True), jnp.max(scores[1], axis=0, keepdims=True))
-        if d > 0:
-            old = peaks[index, 0:1]
-            new = jnp.maximum(old, new)
-        weight = jnp.concatenate([jnp.exp2(part - new).astype(BF16) for part in scores], axis=0)
-        added = dot(latt[:, d * chunk : (d + 1) * chunk], weight)
-        acct[index] = added if d == 0 else acct[index] * jnp.exp2(old - new) + added
-        peaks[index] = jnp.broadcast_to(new, peaks.shape[1:])
+            found.append(dot_nt(keys, qs[v, index, t * tile : (t + 1) * tile, :]))
+        return found
+
+    def attend(*steps):
+        units = [(index, d, t) for index, d in steps for t in range(heads * WINDOW // tile)]
+        later = scores_of(*units[0])
+        held = None
+
+        def blend(index, d, span, weight, old, new):
+            added = dot(latt[:, d * chunk : (d + 1) * chunk], weight)
+            acct[index, :, span] = added if d == 0 else acct[index, :, span] * jnp.exp2(old - new) + added
+
+        for i, (index, d, t) in enumerate(units):
+            scores = later
+            if i + 1 < len(units):
+                later = scores_of(*units[i + 1])
+            span = slice(t * tile, (t + 1) * tile)
+            new = jnp.maximum(jnp.max(scores[0], axis=0, keepdims=True), jnp.max(scores[1], axis=0, keepdims=True))
+            old = None
+            if d > 0:
+                old = peaks[index, 0:1, span]
+                new = jnp.maximum(old, new)
+            peaks[index, 0:1, span] = new
+            weight = jnp.concatenate([jnp.exp2(part - new).astype(BF16) for part in scores], axis=0)
+            if held:
+                blend(*held)
+            held = (index, d, span, weight, old, new)
+        blend(*held)
 
     reach = 3 * WINDOW
     seq_total = rows * n_sp
+    square = jnp.where(
+        lax.broadcasted_iota(jnp.int32, (k_cols, k_cols), 0) == lax.broadcasted_iota(jnp.int32, (k_cols, k_cols), 1),
+        1.0,
+        0.0,
+    ).astype(BF16)
+
+    def flip(spot):
+        where = pl.ds(pl.multiple_of(spot, WINDOW), WINDOW)
+        vt[:, where] = dot_nt(square, halo[where, k_cols:]).astype(BF16)
 
     def window(index):
-        start = block_at[index]
-        spots = lax.broadcasted_iota(jnp.int32, (WINDOW, reach), 0)
-        keys_at = lax.broadcasted_iota(jnp.int32, (WINDOW, reach), 1)
+        h_copies[index].wait_recv()
+        flip((1 - c if index == 0 else c) * (rows + WINDOW))
+        start_at = block_at[index]
+        keys_at = lax.broadcasted_iota(jnp.int32, (reach, WINDOW), 0)
+        spots = lax.broadcasted_iota(jnp.int32, (reach, WINDOW), 1)
         distance = jnp.abs(spots + WINDOW - keys_at)
-        key_pos = sp * rows + start - WINDOW + keys_at
+        key_pos = sp * rows + start_at - WINDOW + keys_at
         inside = (distance <= WINDOW) & (key_pos >= 0) & (key_pos < seq_total)
         gone = jnp.where(inside, distance.astype(F32), jnp.inf)
-        where = pl.ds(pl.multiple_of(start, WINDOW), reach)
+        where = pl.ds(pl.multiple_of(start_at, WINDOW), reach)
+        ones = jnp.ones((ONES, reach), BF16)
         group = 2
-        for kv_head in range(k_cols // DH):
-            keys = halo[where, kv_head * DH : (kv_head + 1) * DH]
-            values = halo[where, k_cols + kv_head * DH : k_cols + (kv_head + 1) * DH]
+        kv_heads = range(k_cols // DH)
+        own_cols = [slice(kv_head * DH, (kv_head + 1) * DH) for kv_head in kv_heads]
+        dots = []
+        for kv_head in kv_heads:
+            query = jnp.concatenate(
+                [qwin[index, :, n * DH : (n + 1) * DH] for n in range(kv_head * group, (kv_head + 1) * group)], axis=0
+            )
+            dots.append(dot_nt(halo[where, own_cols[kv_head]], query))
+        weights, sinks = [], []
+        for kv_head in kv_heads:
+            for j in range(group):
+                head = kv_head * group + j
+                place = (tp * sink_ref.shape[0] + head + 1).astype(F32)
+                slope = jnp.exp2(jnp.full((1, WINDOW), -8.0 / HEADS_A, F32) * place) * LOG2E
+                sink = sink_ref[head] * LOG2E
+                scores = dots[kv_head][:, j * WINDOW : (j + 1) * WINDOW] * (DH ** (-0.5) * LOG2E) - slope * gone
+                peak = jnp.maximum(jnp.max(scores, axis=0, keepdims=True), sink)
+                weights.append(jnp.exp2(scores - peak).astype(BF16))
+                sinks.append(jnp.exp2(sink - peak))
+        blends = []
+        for kv_head in kv_heads:
+            mine_of = slice(kv_head * group, (kv_head + 1) * group)
+            left_side = jnp.concatenate([vt[own_cols[kv_head], where], ones], axis=0)
+            blends.append(dot(left_side, jnp.concatenate(weights[mine_of], axis=1)))
+        for kv_head in kv_heads:
+            bottom = blends[kv_head][DH : DH + 1] + jnp.concatenate(
+                sinks[kv_head * group : (kv_head + 1) * group], axis=1
+            )
+            blended = blends[kv_head][0:DH] / bottom
+            pair = jnp.concatenate([blended[:, j * WINDOW : (j + 1) * WINDOW] for j in range(group)], axis=0)
             first = kv_head * group
-            query = jnp.concatenate(
-                [qwin[index, :, (first + j) * DH : (first + j + 1) * DH] for j in range(group)], axis=0
-            )
-            dots = dot_nt(query, keys) * (DH ** (-0.5) * LOG2E)
-            weights, bottoms = [], []
-            for j in range(group):
-                head = first + j
-                place = (tp * sink_ref.shape[0] + head + 1).astype(F32)
-                slope = jnp.exp2(jnp.full((1, reach), -8.0 / HEADS_A, F32) * place) * LOG2E
-                sink = sink_ref[head] * LOG2E
-                scores = dots[j * WINDOW : (j + 1) * WINDOW] - slope * gone
-                peak = jnp.maximum(jnp.max(scores, axis=1, keepdims=True), sink)
-                weight = jnp.exp2(scores - peak)
-                bottoms.append(jnp.sum(weight, axis=1, keepdims=True) + jnp.exp2(sink - peak))
-                weights.append(weight.astype(BF16))
-            blended = dot(jnp.concatenate(weights, axis=0), values)
-            outs = [blended[j * WINDOW : (j + 1) * WINDOW] / bottoms[j] for j in range(group)]
-            win[index, :, first * DH : (first + group) * DH] = jnp.concatenate(outs, axis=1).astype(BF16)
+            win[index, :, first * DH : (first + group) * DH] = jnp.transpose(pair).astype(BF16)
 
     o_copies, f_copies = [], []
 
     def give(index):
         inverse = 1.0 / acct[index, UNROTATED_WIDTH : UNROTATED_WIDTH + 1, :]
+        flipped = []
         for h in range(heads):
             where = slice(h * WINDOW, (h + 1) * WINDOW)
-            blended = jnp.transpose(acct[index, 0:UNROTATED_WIDTH, where] * inverse[:, where]).astype(BF16)
-            spot = slice(h * VALUE_WIDTH, (h + 1) * VALUE_WIDTH)
-            lat[index, :, spot] = dot(blended, vup[:, spot]).astype(BF16)
+            flipped.append(jnp.transpose(acct[index, 0:UNROTATED_WIDTH, where] * inverse[:, where]).astype(BF16))
+        lats = jnp.concatenate(
+            [dot(flipped[h], vup[:, h * VALUE_WIDTH : (h + 1) * VALUE_WIDTH]).astype(BF16) for h in range(heads)],
+            axis=1,
+        )
+        wins = win[index]
 
         def terms(j):
             where = pl.ds(pl.multiple_of(j * cols, cols), cols)
-            return dot(win[index], ow[:, where]) + dot(lat[index], ol[:, where])
+            return dot(wins, ow[:, where]) + dot(lats, ol[:, where])
 
         where = pl.ds(pl.multiple_of(block_at[index], WINDOW), WINDOW)
         for s, other in others:
@@ -402,66 +484,92 @@
         f_copies.append(copy)
 
     both = range(parts)
-    for g in both:
-        got_y(0, g)
-        if hi > 1:
-            got_z(1, g)
-    arrive(0)
-    keys_values(0)
-    for load in loads[11:]:
-        load.wait()
-    queries(0)
-    ready(0)
+    last = hi - 1
+
+    def events(*todo):
+        for got, d in todo:
+            for g in both:
+                got(d, g)
+
+    def on(role, todo):
+        @pl.when(inner if role else jnp.logical_not(inner))
+        def _():
+            for got, d in todo:
+                for g in both:
+                    if got is got_z:
+                        got_z(d, g, role)
+                    else:
+                        got(d, g)
+
+    def inside_z(*todo):
+        on(True, todo)
+
+    def outside_z(*todo):
+        on(False, todo)
+
     if relayed:
         for g in both:
-            got_z(2, g)
-        attend(0, 0)
-        for g in both:
-            got_y(1, g)
-            got_z(3, g)
+            got_y(0, g)
+            got_z(1, g)
+        inside_z((got_z, 2), (got_z, 3))
+        ready(0)
+        arrive(0)
+        keys_values(0)
+        inside_z((got_y, 1))
+        for load in loads[11:]:
+            load.wait()
+        queries(0)
+        attend((0, 0))
+        inside_z((got_y, 2))
+        outside_z((got_y, 1), (got_z, 2))
         ready(1)
-        attend(0, 1)
+        attend((0, 1))
+        inside_z((got_y, 3))
+        outside_z((got_z, 3))
         arrive(1)
         keys_values(1)
-        for g in both:
-            got_y(2, g)
-        h_copies[0].wait_recv()
+        outside_z((got_y, 2))
         window(0)
-        for g in both:
-            got_y(3, g)
+        queries(1)
         ready(2)
-        attend(0, 2)
-        ready(3)
-        attend(0, 3)
+        outside_z((got_y, 3))
+        attend((0, 2))
     else:
-        attend(0, 0)
         for d in range(1, hi):
-            for g in both:
-                got_y(d, g)
-                if d + 1 < hi:
-                    got_z(d + 1, g)
+            events((got_y, d - 1), (got_z, d))
+        events((got_y, last))
+        arrive(0)
+        keys_values(0)
+        for load in loads[11:]:
+            load.wait()
+        queries(0)
+        for d in range(last - 1):
             ready(d)
-            attend(0, d)
+            attend((0, d))
+        ready(last - 1)
         arrive(1)
         keys_values(1)
-        h_copies[0].wait_recv()
         window(0)
+        queries(1)
+        attend((0, last - 1))
+    ready(last)
+    attend((0, last))
     give(0)
-    queries(1)
-    for d in range(hi):
-        attend(1, d)
-    h_copies[1].wait_recv()
     window(1)
+    attend(*[(1, d) for d in range(hi)])
     give(1)
 
-    for copy in list(x_copies.values()) + s_copies + list(p_copies.values()) + sends + h_copies:
+    for copy in list(x_copies.values()) + s_copies + list(p_copies.values()) + h_copies:
         copy.wait_send()
+    for make in sent.values():
+        make().wait_send()
     if relayed:
 
         @pl.when(inner)
         def _():
-            for copy in relays:
-                copy.wait_send()
+            for d in (2, 3):
+                for g in both:
+                    relay(d, g).wait_send()
 
     for copy in f_copies + o_copies:
         copy.wait()
@@ -533,14 +641,14 @@
             vmem((2, blocks, span, 2 * UNROTATED_WIDTH)),
             vmem((blocks, WINDOW, win_query.shape[1])),
             vmem((rows + 2 * WINDOW, 2 * win_key.shape[1])),
+            vmem((win_key.shape[1], rows + 2 * WINDOW)),
             vmem((blocks, UNROTATED_WIDTH + ONES, span), F32),
             vmem((blocks, 8, span), F32),
             vmem((blocks, WINDOW, heads_a * DH)),
-            vmem((blocks, WINDOW, heads_l * VALUE_WIDTH)),
             vmem((blocks, n_tp - 1, WINDOW, cols)),
             vmem((blocks, WINDOW, cols), F32),
             dma((len(operands),)),
-            dma((n_tp, 3)), dma((n_tp, 3)),
+            dma((n_tp, 2)), dma((n_tp, 2)),
             dma((n_tp,)), dma((n_tp,)),
             dma((n_tp, parts)), dma((n_tp, parts)),
             dma((hi, parts)), dma((hi, parts)),
@@ -549,6 +657,7 @@
             dma((2,)), dma((2,)),
             dma((blocks, n_tp)), dma((blocks, n_tp)),
             dma((blocks,)),
+            pltpu.SemaphoreType.REGULAR,
         ],
         compiler_params=pltpu.CompilerParams(
             collective_id=0, has_side_effects=True, vmem_limit_bytes=60 * 1024 * 1024

time: 48.9 us -> 43.7 us (0.89)
  Pallas kernels: 46.4 us -> 41.2 us
    pallas_call x1, Pallas kernels: 46.4 us -> 41.2 us  [per_device(): pl.pallas_call(functools.partial(layer_kernel, n_sp, n_tp, parts), out_sh...]
where the time goes in v2:
time: 43.7 us; the launch traced here: 43.5 us
  Pallas kernels  41.2 us (94%)
  other arithmetic  2.3 us (5%)
    pallas_call x1, Pallas kernels, per_device(): pl.pallas_call(functools.partial(layer_kernel, n_sp, n_tp, parts), out_sh...  41.2 us
    convert_element_type x1, other arithmetic, per_device(): return total.astype(BF16)  2.3 us

profile of v2, /device:TPU:0, one launch (start us, length us, event | category | flops | bytes accessed | tf_op | source)
XLA Modules:
  0.0 43.5 jit_solution(17499211041927905580)
XLA Ops:
  0.0 41.2 %layer.1 = (f32[256,1024]{1,0:T(8,128)}, bf16[1,256,1024]{2,1,0:T(8,128)(2,1)}) custom-call(f32[8]{0:T(128)} %sink_ref.1, bf16[256,1024]{1,0:T(8,128)(2,1)} %x_hbm.1, f32[2,1,1024]{2,1,0:T(1,128)} %bitcast.7, f32[2,256,64]{2,1,0:T(8,128)} %constant.4.clone.near_hbm, f32[16,2,64]{2,1,0:T(2,128)} %constant.5.clone.base_hbm, f32[1,128]{1,0:T(1,128)} %bitcast.8, ...), custom_call_target="tpu_custom_call" | custom-call | tf_op jit(solution)/shard_map/layer/pallas_call | solution.py:614
  41.2 2.3 %fusion = bf16[256,1024]{1,0:T(8,128)(2,1)} fusion(f32[256,1024]{1,0:T(8,128)} %get-tuple-element.7, bf16[1,256,1024]{2,1,0:T(8,128)(2,1)} %get-tuple-element.8), kind=kLoop, calls=%fused_computation.1 | loop fusion | flops 786432 | bytes 2097152 | tf_op jit(solution)/shard_map/convert_element_type | solution.py:670
